TPU v7x, 256 devices: a whole 4x4x8 slice. The times are simulated.
256 devices in a mesh: ep: 64 (over z, y, core), tp: 4 (over x).
Axes of the slice: x: 4, y: 4, z: 8, core: 2. Of those that a mesh axis runs over, the one named last changes fastest.
Arguments:
- mixer_input: bfloat16 [32768, 2048], P(('ep', 'tp')), may hold values from -6 to 6
- expert_input: bfloat16 [32768, 2048], P(('ep', 'tp')), may hold values from -6 to 6
- mixer_gain: float32 [2048], replicated, may hold values from 0.1 to 1.9
- expert_gain: float32 [2048], replicated, may hold values from 0.1 to 1.9
- query_weight: bfloat16 [2048, 1024], P(None, 'tp'), may hold values from -0.125 to 0.125
- key_weight: bfloat16 [2048, 1024], P(None, 'tp'), may hold values from -0.125 to 0.125
- value_weight: bfloat16 [2048, 1024], P(None, 'tp'), may hold values from -0.125 to 0.125
- out_weight: bfloat16 [1024, 2048], P('tp'), may hold values from -0.1875 to 0.1875
- decay_rate: float32 [8], P('tp'), may hold values from 0 to 0.12
- routing: int32 [32768, 4], P('ep'), may hold values from 0 to 63, all different within a row; in each aligned block of 128 rows (0 to 127, 128 to 255, ...) at most 12 rows name the same one
- route_weight: float32 [32768, 4], P('ep'), may hold values from 0.2 to 1
- gate_weight: bfloat16 [64, 2048, 1024], P('ep', None, 'tp'), may hold values from -0.125 to 0.125
- up_weight: bfloat16 [64, 2048, 1024], P('ep', None, 'tp'), may hold values from -0.125 to 0.125
- down_weight: bfloat16 [64, 1024, 2048], P('ep', None, 'tp'), may hold values from -0.1875 to 0.1875
- shared_gate: bfloat16 [2048, 512], P(None, 'tp'), may hold values from -0.125 to 0.125
- shared_up: bfloat16 [2048, 512], P(None, 'tp'), may hold values from -0.125 to 0.125
- shared_down: bfloat16 [512, 2048], P(None, 'tp'), may hold values from -0.25 to 0.25
Outputs:
- mixer_output: float32 [32768, 2048], P(('ep', 'tp'))
- expert_output: float32 [32768, 2048], P('ep', 'tp')
Inputs may be any that keep to these rules, and one draw needn't show every extreme that they name: `routing`: each row names 4 different experts. In each aligned block of 128 rows, no expert is named by more than 12 rows, and in some blocks one expert is named by exactly 12 rows.
All inputs are finite; a program needn't handle non-finite values.
Results may differ from a plain program's by a relative error of at most 0.0095.
Values may be sent and summed in bfloat16 or wider, within the bound.
A program may use at most 128 MiB of HBM per device.

v0:
```python
import jax
import jax.numpy as jnp
from jax import lax
from jax.sharding import Mesh
from jax.sharding import PartitionSpec as P

HD = 128
BLK = 64
EP = ("ep_0", "ep_1", "ep_2")
EP_TP = ("ep_0", "ep_1", "ep_2", "tp")
NORM_EPS = 1e-06
ROPE_BASE = 10000.0
EXACT_MATMUL = lax.Precision.HIGHEST


def nothing_yet(value, identity):
    return jax.tree.map(
        lambda a, e: jnp.broadcast_to(jnp.asarray(e, a.dtype), a.shape), value, identity
    )


def entering_2(value, axes, combine, identity):
    before = start = nothing_yet(value, identity)
    subtotal = value
    for axis in reversed(axes):
        count, mine = (lax.axis_size(axis), lax.axis_index(axis))
        pieces = jax.tree.map(lambda part: lax.all_gather(part, axis), subtotal)
        inside, subtotal = (start, start)
        for k in range(count):
            passed = k < mine
            subtotal = combine(subtotal, jax.tree.map(lambda part: part[k], pieces))
            inside = jax.tree.map(lambda new, old: jnp.where(passed, new, old), subtotal, inside)
        before = combine(inside, before)
    return before


def sent_together(arrays, axis, dim, along):
    ends, at = ([], 0)
    for a in arrays[:-1]:
        at += a.shape[along]
        ends.append(at)
    both = jnp.concatenate(arrays, axis=along)
    return tuple(jnp.split(lax.all_gather(both, axis, axis=dim, tiled=True), ends, axis=along))


def norm_rows(inputs, gain_vector):
    values = inputs.astype(jnp.float32)
    scaled = values * lax.rsqrt(jnp.mean(values * values, axis=-1, keepdims=True) + NORM_EPS)
    return (scaled * gain_vector).astype(jnp.bfloat16)


def rotate(head_rows, positions):
    head_size = head_rows.shape[-1]
    inverse = ROPE_BASE ** (-jnp.arange(0, head_size, 2, dtype=jnp.float32) / head_size)
    angles = positions[:, None] * inverse[None, :]
    cosine = jnp.cos(angles)[:, None, :]
    sine_part = jnp.sin(angles)[:, None, :]
    front_half = head_rows[..., : head_size // 2]
    behind = head_rows[..., head_size // 2 :]
    return jnp.concatenate(
        [front_half * cosine - behind * sine_part, front_half * sine_part + behind * cosine],
        axis=-1,
    )


def project(inputs, weight, head_total):
    product = jnp.dot(inputs, weight, preferred_element_type=jnp.float32).astype(jnp.bfloat16)
    product = lax.optimization_barrier(product)
    return product.astype(jnp.float32).reshape(inputs.shape[0], head_total, -1)


def chain_combine(earlier, latter):
    return (earlier[0] * latter[0], latter[0][:, None, None] * earlier[1] + latter[1])


def retain_local(query_heads, key_heads, value_heads, decay_rates):
    length, head_total, head_size = query_heads.shape
    blocks = length // BLK
    log_gamma = -decay_rates
    inner_pos = jnp.arange(BLK, dtype=jnp.float32)
    offsets = inner_pos[:, None] - inner_pos[None, :]
    inside_block_output = jnp.where(
        offsets >= 0, jnp.exp(log_gamma[:, None, None] * jnp.maximum(offsets, 0.0)), 0.0
    )
    key_scale = jnp.exp(log_gamma[None, :] * (BLK - 1.0 - inner_pos)[:, None])
    query_scale = jnp.exp(log_gamma[None, :] * (inner_pos + 1.0)[:, None])
    blocked = (blocks, BLK, head_total, head_size)
    q_blocks = query_heads.reshape(blocked)
    k_blocks = key_heads.reshape(blocked)
    v_blocks = value_heads.reshape(blocked)
    attention_scores = (
        jnp.einsum("nchd,nmhd->nhcm", q_blocks, k_blocks, precision=EXACT_MATMUL)
        * inside_block_output[None]
    )
    nearby = jnp.einsum("nhcm,nmhe->nche", attention_scores, v_blocks, precision=EXACT_MATMUL)
    block_states = jnp.einsum(
        "nchd,nche->nhde", k_blocks * key_scale[None, :, :, None], v_blocks, precision=EXACT_MATMUL
    )
    block_offset_rows = jnp.arange(blocks, dtype=jnp.float32)
    to_end = jnp.exp(log_gamma[None, :] * BLK * (blocks - 1.0 - block_offset_rows)[:, None])
    summary = jnp.einsum("nh,nhde->hde", to_end, block_states, precision=EXACT_MATMUL)
    through = jnp.exp(log_gamma * (BLK * blocks))
    incoming = entering_2(
        (through, summary), EP, chain_combine, (jnp.ones_like(through), jnp.zeros_like(summary))
    )[1]
    block_gaps = block_offset_rows[:, None] - 1.0 - block_offset_rows[None, :]
    carry_mix = jnp.where(
        block_gaps >= 0, jnp.exp(log_gamma[:, None, None] * BLK * jnp.maximum(block_gaps, 0.0)), 0.0
    )
    entering = jnp.einsum("hbj,jhde->bhde", carry_mix, block_states, precision=EXACT_MATMUL)
    entering = (
        entering
        + jnp.exp(log_gamma[None, :] * BLK * block_offset_rows[:, None])[:, :, None, None]
        * incoming[None]
    )
    distant = jnp.einsum(
        "bchd,bhde->bche",
        q_blocks * query_scale[None, :, :, None],
        entering,
        precision=EXACT_MATMUL,
    )
    retained = (nearby + distant).reshape(length, head_total, head_size)
    normed = retained * lax.rsqrt(jnp.mean(retained * retained, axis=-1, keepdims=True) + NORM_EPS)
    return normed.astype(jnp.bfloat16).reshape(length, head_total * head_size)


def assign_slots(routes, source_rows, capacity, expert_count):
    token_count, pick_count = routes.shape
    chosen = routes.reshape(token_count * pick_count)
    onehot = (chosen[:, None] == jnp.arange(expert_count, dtype=jnp.int32)[None, :]).astype(
        jnp.int32
    )
    per_source = onehot.reshape(token_count // source_rows, source_rows * pick_count, expert_count)
    earlier_hits = jnp.cumsum(per_source, axis=1) - per_source
    ranks = jnp.sum(earlier_hits * per_source, axis=2).reshape(token_count * pick_count)
    sources = jnp.arange(token_count * pick_count, dtype=jnp.int32) // (source_rows * pick_count)
    return (chosen, sources * capacity + ranks)


def gather_slots(token_rows, chosen, slot_ids, slot_count, expert_count, pick_count):
    owners = jnp.arange(chosen.shape[0], dtype=jnp.int32) // pick_count + 1
    owner_table = jnp.zeros((slot_count, expert_count), jnp.int32).at[slot_ids, chosen].set(owners)
    padded = jnp.concatenate(
        [jnp.zeros((1, token_rows.shape[1]), token_rows.dtype), token_rows], axis=0
    )
    return padded[owner_table]


def expert_hidden(routed_rows, gate_weight, up_weight):
    per_device = gate_weight.shape[0]
    grouped = routed_rows.reshape(
        routed_rows.shape[0], routed_rows.shape[1] // per_device, per_device, routed_rows.shape[2]
    )
    gate_part = jnp.einsum(
        "snxd,xdf->snxf", grouped, gate_weight, preferred_element_type=jnp.float32
    )
    up_part = jnp.einsum("snxd,xdf->snxf", grouped, up_weight, preferred_element_type=jnp.float32)
    return (jax.nn.silu(gate_part) * up_part).astype(jnp.bfloat16)


def shards(
    mixer_input,
    expert_input,
    mixer_gain,
    expert_gain,
    query_weight,
    key_weight,
    value_weight,
    out_weight,
    decay_rate,
    routing,
    route_weight,
    gate_weight,
    up_weight,
    down_weight,
    shared_gate,
    shared_up,
    shared_down,
):
    own_count = mixer_input.shape[0]
    tp_index = lax.axis_index("tp")
    own_expert_rows = norm_rows(expert_input, expert_gain)
    mixer_rows, expert_rows = sent_together(
        (norm_rows(mixer_input, mixer_gain), own_expert_rows), "tp", 0, 1
    )
    group_count = mixer_rows.shape[0]
    head_total = decay_rate.shape[0]
    positions = (
        lax.axis_index(EP) * group_count + jnp.arange(group_count, dtype=jnp.int32)
    ).astype(jnp.float32)
    query_heads = rotate(project(mixer_rows, query_weight, head_total), positions) * HD ** (-0.5)
    key_heads = rotate(project(mixer_rows, key_weight, head_total), positions)
    value_heads = project(mixer_rows, value_weight, head_total)
    mixed_heads = retain_local(query_heads, key_heads, value_heads, decay_rate)
    mixer_output = lax.psum_scatter(
        jnp.dot(mixed_heads, out_weight, preferred_element_type=jnp.float32).astype(jnp.bfloat16),
        "tp",
        scatter_dimension=0,
        tiled=True,
    ).astype(jnp.float32)
    expert_count = lax.axis_size(EP) * gate_weight.shape[0]
    pick_count = routing.shape[1]
    capacity = (3 * own_count * pick_count + 2 * expert_count - 1) // (2 * expert_count)
    chosen, slot_ids = assign_slots(routing, own_count, capacity, expert_count)
    own_span = own_count * pick_count
    own_chosen = lax.dynamic_slice_in_dim(chosen, tp_index * own_span, own_span, 0)
    own_slots = (
        lax.dynamic_slice_in_dim(slot_ids, tp_index * own_span, own_span, 0) - tp_index * capacity
    )
    outgoing = gather_slots(
        own_expert_rows, own_chosen, own_slots, capacity, expert_count, pick_count
    )
    arrived = lax.all_to_all(outgoing, EP, split_axis=1, concat_axis=1, tiled=True)
    hidden = expert_hidden(
        lax.all_gather(arrived, "tp", axis=0, tiled=True), gate_weight, up_weight
    )
    shared_hidden = (
        jax.nn.silu(jnp.dot(expert_rows, shared_gate, preferred_element_type=jnp.float32))
        * jnp.dot(expert_rows, shared_up, preferred_element_type=jnp.float32)
    ).astype(jnp.bfloat16)
    full_hidden, full_shared = (
        lax.all_gather(hidden, "tp", axis=3, tiled=True),
        lax.all_gather(shared_hidden, "tp", axis=1, tiled=True),
    )
    results = jnp.einsum(
        "snxf,xfe->snxe", full_hidden, down_weight, preferred_element_type=jnp.float32
    ).astype(jnp.bfloat16)
    results = results.reshape(results.shape[0], expert_count, results.shape[3])
    returned = lax.all_to_all(results, EP, split_axis=1, concat_axis=1, tiled=True)
    flat_results = returned.reshape(returned.shape[0] * expert_count, returned.shape[2])
    picked = flat_results[slot_ids * expert_count + chosen].astype(jnp.float32)
    weighted = jnp.sum(
        picked.reshape(group_count, pick_count, -1) * route_weight[:, :, None], axis=1
    )
    shared_result = jnp.dot(full_shared, shared_down, preferred_element_type=jnp.float32)
    expert_output = weighted + shared_result
    return (mixer_output, expert_output)


def solution(mesh):
    finer = Mesh(mesh.devices.reshape(8, 4, 2, mesh.shape["tp"]), ("ep_0", "ep_1", "ep_2", "tp"))
    placed = (
        P(EP_TP, None),
        P(EP_TP, None),
        P(),
        P(),
        P(None, "tp"),
        P(None, "tp"),
        P(None, "tp"),
        P("tp", None),
        P("tp"),
        P(EP, None),
        P(EP, None),
        P(EP, None, "tp"),
        P(EP, None, "tp"),
        P(EP, None, "tp"),
        P(None, "tp"),
        P(None, "tp"),
        P(None, "tp"),
    )
    return jax.shard_map(
        shards,
        mesh=finer,
        in_specs=placed,
        out_specs=(P(EP_TP, None), P(EP, "tp")),
        check_vma=False,
    )
```

profile of v0, /device:TPU:8, one launch (start us, length us, event | category | flops | bytes accessed | tf_op | source)
XLA Modules:
  0.0 539.4 jit_solution(6858122981832166352)
XLA Ops:
  11.3 4.8 reduce-window.6
  17.0 25.4 %scatter_fusion = s32[12,64]{1,0:T(8,128)S(1)} fusion(s32[12,64]{1,0:T(8,128)S(1)} %broadcast.456, s32[512]{0:T(512)S(1)} %bitcast.156, s32[512]{0:T(512)S(1)} %fusion.96), kind=kCustom, calls=%fused_computation.2 | custom fusion | bytes 10240 | tf_op jit(solution)/shard_map/scatter | solution.py:142
  43.6 4.3 gather_fusion
  47.9 3.7 copy.112
  51.5 108.1 %all_to_all.10 = bf16[12,64,2048]{2,0,1:T(8,128)(2,1)S(1)} all-to-all(bf16[12,64,2048]{2,0,1:T(8,128)(2,1)S(1)} %copy.112), channel_id=1, replica_groups=mesh['ep_0'=8,'ep_1'=4,'ep_2'=2,'tp'=4] {'ep_0','ep_1','ep_2'}, dimensions={1} | all-to-all | bytes 6291456 | tf_op jit(solution)/shard_map/all_to_all | solution.py:213
  159.6 3.4 copy.113
  165.6 114.8 %all-gather.13.cloned.1.call-done = bf16[48,64,2048]{2,1,0:T(8,128)(2,1)} async-done(((bf16[12,64,2048]{2,1,0:T(8,128)(2,1)}), bf16[48,64,2048]{2,1,0:T(8,128)(2,1)}) %all-gather.13.cloned.1.call-update) | async-done | bytes 12582928 | tf_op jit(solution)/shard_map/all_gather | solution.py:215
  280.4 7.9 %fusion.43 = f32[48,64,256]{2,1,0:T(8,128)S(1)} fusion(bf16[48,64,2048]{2,1,0:T(8,128)(2,1)} %all-gather.13.cloned.1.call-done, bf16[1,2048,256]{2,1,0:T(8,128)(2,1)} %param.29), kind=kOutput, calls=%fused_computation.48 | convolution fusion | flops 3221225472 | bytes 16777216 | tf_op jit(solution)/shard_map/snxd,xdf->snxf/dot_general | solution.py:157
  288.9 5.2 fusion.2
  299.4 8.6 %all-reduce.2 = f32[8]{0:T(128)S(1)} all-reduce(f32[8]{0:T(128)S(1)} %get-tuple-element.36), channel_id=4, replica_groups=mesh['ep_0'=8,'ep_1'=4,'ep_2'=2,'tp'=4] {'ep_1'}, use_global_device_ids=true, to_apply=%add.2 | all-reduce | flops 8 | bytes 64
  308.7 16.6 %all-gather.3 = f32[8,1,2]{2,1,0:T(1,128)S(1)} all-gather(f32[1,1,2]{2,1,0:T(1,128)S(1)} %get-tuple-element.28), channel_id=1, replica_groups=mesh['ep_0'=8,'ep_1'=4,'ep_2'=2,'tp'=4] {'ep_0'}, dimensions={0}, use_global_device_ids=true | all-gather | bytes 72 | tf_op jit(solution)/shard_map/all_gather | solution.py:27
  329.1 5.5 %all-gather.9.cloned.1.call-done = bf16[512,4096]{1,0:T(8,128)(2,1)} async-done(((bf16[128,4096]{1,0:T(8,128)(2,1)}), bf16[512,4096]{1,0:T(8,128)(2,1)}) %all-gather.9.cloned.1.call-update) | async-done | bytes 4194320 | tf_op jit(solution)/shard_map/all_gather | solution.py:43
  351.2 12.8 %all_gather.47 = f32[4,2,128,128]{3,2,1,0:T(8,128)S(1)} all-gather(f32[1,2,128,128]{3,2,1,0:T(8,128)S(1)} %fusion.72), channel_id=1, replica_groups=mesh['ep_0'=8,'ep_1'=4,'ep_2'=2,'tp'=4] {'ep_1'}, dimensions={0}, use_global_device_ids=true | all-gather | bytes 655360 | tf_op jit(solution)/shard_map/all_gather | solution.py:27
  364.9 43.6 %all-gather.15.cloned.1.call-done = bf16[48,64,1,1024]{3,1,0,2:T(8,128)(2,1)} async-done(((bf16[48,64,1,256]{3,1,0,2:T(8,128)(2,1)}), bf16[48,64,1,1024]{3,1,0,2:T(8,128)(2,1)}) %all-gather.15.cloned.1.call-update) | async-done | bytes 6291472 | tf_op jit(solution)/shard_map/all_gather | solution.py:222
  408.5 6.4 %fusion.6 = bf16[48,64,512]{2,1,0:T(8,128)(2,1)S(1)} fusion(bf16[48,64,1,1024]{3,1,0,2:T(8,128)(2,1)} %all-gather.15.cloned.1.call-done, bf16[1,1024,512]{2,1,0:T(8,128)(2,1)S(1)} %copy-done), kind=kOutput, calls=%fused_computation.14 | convolution fusion | flops 3222798336 | bytes 10485760 | tf_op jit(solution)/shard_map/snxf,xfe->snxe/dot_general | solution.py:225
  414.9 3.4 copy.114
  418.3 10.9 %all-to-all-start.1 = ((bf16[48,64,512]{2,0,1:T(8,128)(2,1)}), bf16[48,64,512]{2,0,1:T(8,128)(2,1)}, u32[]{:S(2)}, u32[]{:S(2)}) async-start(bf16[48,64,512]{2,0,1:T(8,128)(2,1)} %copy.114), calls=%async_computation.2 | async-start | bytes 6291456 | tf_op jit(solution)/shard_map/all_to_all | solution.py:229
  434.5 24.3 %all-gather.11.cloned.1.call-done = f32[8,2,128,128]{3,2,1,0:T(8,128)} async-done(((f32[1,2,128,128]{3,2,1,0:T(8,128)}), f32[8,2,128,128]{3,2,1,0:T(8,128)}) %all-gather.11.cloned.1.call-update) | async-done | bytes 1048592 | tf_op jit(solution)/shard_map/all_gather | solution.py:27
  465.0 3.4 convolution_convert_fusion
  473.4 18.1 %all_gather.51 = bf16[512,512]{1,0:T(8,128)(2,1)} all-gather(bf16[512,128]{1,0:T(8,128)(2,1)S(1)} %fusion.33), channel_id=1, replica_groups=mesh['ep_0'=8,'ep_1'=4,'ep_2'=2,'tp'=4] {'tp'}, dimensions={1}, use_global_device_ids=true | all-gather | bytes 655360 | tf_op jit(solution)/shard_map/all_gather | solution.py:223
  491.5 12.0 %reduce-scatter.2.cloned.1.call-done = bf16[128,2048]{1,0:T(8,128)(2,1)} async-done(((bf16[512,2048]{1,0:T(8,128)(2,1)}), bf16[128,2048]{1,0:T(8,128)(2,1)}) %reduce-scatter.2.cloned.1.call-update) | async-done | bytes 524304 | tf_op jit(solution)/shard_map/reduce_scatter | solution.py:195
  508.1 5.3 copy.115
  513.4 9.9 %gather_fusion.1 = bf16[2048,512]{1,0:T(8,128)(2,1)S(1)} fusion(bf16[3072,512]{1,0:T(8,128)(2,1)} %bitcast.155, s32[2048]{0:T(1024)S(1)} %broadcast_clamp_fusion), kind=kCustom, calls=%fused_computation.1 | custom fusion | bytes 4202496 | tf_op jit(solution)/shard_map/gather | solution.py:231
  526.3 4.9 multiply_reduce_fusion
  (166 shorter events, 60.2 us)
Async XLA Ops:
  7.2 401.3 %copy-start = (bf16[1,1024,512]{2,1,0:T(8,128)(2,1)S(1)}, bf16[1,1024,512]{2,1,0:T(8,128)(2,1)}, u32[]{:S(2)}) copy-start(bf16[1,1024,512]{2,1,0:T(8,128)(2,1)} %param.30) | copy-start | bytes 3145732
  7.2 273.3 %all-gather.13.cloned.1.call-start = ((), (), s32[]{:S(2)}) async-start(), calls=%async_computation.6 | async-start | bytes 15728640 | tf_op jit(solution)/shard_map/all_gather | solution.py:215
  11.2 31.2 %copy-start.6 = (bf16[128,2048]{1,0:T(8,128)(2,1)S(1)}, bf16[128,2048]{1,0:T(8,128)(2,1)}, u32[]{:S(2)}) copy-start(bf16[128,2048]{1,0:T(8,128)(2,1)} %param.17) | copy-start | bytes 1572868
  11.2 31.2 %copy-start.12 = (f32[2048]{0:T(1024)S(1)}, f32[2048]{0:T(1024)}, u32[]{:S(2)}) copy-start(f32[2048]{0:T(1024)} %param.19) | copy-start | bytes 24580
  11.2 31.2 %copy-start.13 = (f32[2048]{0:T(1024)S(1)}, f32[2048]{0:T(1024)}, u32[]{:S(2)}) copy-start(f32[2048]{0:T(1024)} %param.20) | copy-start | bytes 24580
  163.0 171.6 %all-gather.9.cloned.1.call-start = ((), (), s32[]{:S(2)}) async-start(), calls=%async_computation.3 | async-start | bytes 5242880 | tf_op jit(solution)/shard_map/all_gather | solution.py:43
  165.1 123.3 %copy-start.32 = (bf16[1,2048,256]{2,1,0:T(8,128)(2,1)S(1)}, bf16[1,2048,256]{2,1,0:T(8,128)(2,1)}, u32[]{:S(2)}) copy-start(bf16[1,2048,256]{2,1,0:T(8,128)(2,1)} %param.28) | copy-start | bytes 3145732
  165.1 243.4 %all-gather.15.cloned.1.call-start = ((), (), s32[]{:S(2)}) async-start(), calls=%async_computation.7 | async-start | bytes 7864320 | tf_op jit(solution)/shard_map/all_gather | solution.py:222
  294.1 164.7 %all-gather.11.cloned.1.call-start = ((), (), s32[]{:S(2)}) async-start(), calls=%async_computation.4 | async-start | bytes 1179648 | tf_op jit(solution)/shard_map/all_gather | solution.py:27
  295.5 41.7 %copy-start.15 = (f32[2]{0:T(128)}, f32[2]{0:T(128)S(1)}, u32[]{:S(2)}) copy-start(f32[2]{0:T(128)S(1)} %get-tuple-element.39) | copy-start | bytes 28
  418.3 89.7 %all-to-all-start.1 = ((bf16[48,64,512]{2,0,1:T(8,128)(2,1)}), bf16[48,64,512]{2,0,1:T(8,128)(2,1)}, u32[]{:S(2)}, u32[]{:S(2)}) async-start(bf16[48,64,512]{2,0,1:T(8,128)(2,1)} %copy.114), calls=%async_computation.2 | async-start | bytes 6291456 | tf_op jit(solution)/shard_map/all_to_all | solution.py:229
  429.2 29.6 %copy-start.19 = (f32[2]{0:T(128)S(1)}, f32[2]{0:T(128)}, u32[]{:S(2)}) copy-start(f32[2]{0:T(128)} %get-tuple-element.31) | copy-start | bytes 28
  429.2 29.6 %copy-start.20 = (f32[2]{0:T(128)S(1)}, f32[2]{0:T(128)}, u32[]{:S(2)}) copy-start(f32[2]{0:T(128)} %get-tuple-element.32) | copy-start | bytes 28
  429.2 29.6 %copy-start.21 = (f32[2]{0:T(128)S(1)}, f32[2]{0:T(128)}, u32[]{:S(2)}) copy-start(f32[2]{0:T(128)} %get-tuple-element.14) | copy-start | bytes 28
  429.2 29.6 %copy-start.22 = (f32[2]{0:T(128)S(1)}, f32[2]{0:T(128)}, u32[]{:S(2)}) copy-start(f32[2]{0:T(128)} %get-tuple-element.15) | copy-start | bytes 28
  429.2 29.6 %copy-start.23 = (f32[2]{0:T(128)S(1)}, f32[2]{0:T(128)}, u32[]{:S(2)}) copy-start(f32[2]{0:T(128)} %get-tuple-element.16) | copy-start | bytes 28
  429.3 29.6 %copy-start.24 = (f32[2]{0:T(128)S(1)}, f32[2]{0:T(128)}, u32[]{:S(2)}) copy-start(f32[2]{0:T(128)} %get-tuple-element.17) | copy-start | bytes 28
  429.3 29.6 %copy-start.25 = (f32[2]{0:T(128)S(1)}, f32[2]{0:T(128)}, u32[]{:S(2)}) copy-start(f32[2]{0:T(128)} %get-tuple-element.18) | copy-start | bytes 28
  429.3 29.6 %copy-start.26 = (f32[2]{0:T(128)S(1)}, f32[2]{0:T(128)}, u32[]{:S(2)}) copy-start(f32[2]{0:T(128)} %get-tuple-element.19) | copy-start | bytes 28
  429.3 31.4 %copy-start.16 = (f32[2]{0:T(128)S(1)}, f32[2]{0:T(128)}, u32[]{:S(2)}) copy-start(f32[2]{0:T(128)} %copy-done.15) | copy-start | bytes 28
  429.3 31.4 %copy-start.18 = (f32[8,2]{0,1:T(2,128)S(1)}, f32[8,2]{0,1:T(2,128)}, u32[]{:S(2)}) copy-start(f32[8,2]{0,1:T(2,128)} %get-tuple-element.26) | copy-start | bytes 196
  429.3 74.2 %reduce-scatter.2.cloned.1.call-start = ((), (), s32[]{:S(2)}) async-start(), calls=%async_computation.5 | async-start | bytes 2621440 | tf_op jit(solution)/shard_map/reduce_scatter | solution.py:195
  432.3 30.1 %copy-start.1 = (f32[512,2,64]{2,0,1:T(8,128)S(1)}, f32[512,2,64]{2,0,1:T(8,128)}, u32[]{:S(2)}) copy-start(f32[512,2,64]{2,0,1:T(8,128)} %get-tuple-element.4) | copy-start | bytes 786436
  432.3 30.1 %copy-start.17 = (f32[64,2]{0,1:T(2,128)S(1)}, f32[64,2]{0,1:T(2,128)}, u32[]{:S(2)}) copy-start(f32[64,2]{0,1:T(2,128)} %get-tuple-element.24) | copy-start | bytes 1540
  (19 other events, 139.9 us)
Sparse Core Ops, SparseCore 0:
  163.1 117.2 all-gather.12
  282.8 51.7 all-gather.8
  336.4 72.0 all-gather.14
  410.1 48.6 all-gather.10
  468.5 34.9 reduce-scatter.1
where the time goes:
time: 547 us; the launch traced here: 539 us
  waiting for transfers between devices  203 us (37%)
  blocking collectives  169 us (31%)
  local copies, waits for them, and re-layouts  67.4 us (12%)
  matrix products  46.5 us (9%)
  other arithmetic  26.2 us (5%)
  between operations  16.1 us (3%)
  starting transfers between devices  11.5 us (2%)
    all_gather x1, waiting for transfers between devices, shards(): lax.all_gather(arrived, 'tp', axis=0, tiled=True)  115 us
    all_to_all x1, blocking collectives, shards(): lax.all_to_all(outgoing, EP, split_axis=1, concat_axis=1, tiled=True)  108 us
    all_gather x1, waiting for transfers between devices, shards(): lax.all_gather(hidden, 'tp', axis=3, tiled=True)  43.6 us
    all_gather x3, blocking collectives, entering_2(): pieces = jax.tree.map(lambda part: lax.all_gather(part, axis), subtotal)  31.6 us
    scatter x1, local copies, waits for them, and re-layouts, gather_slots(): jnp.zeros((slot_count, expert_count), jnp.int32).at[slot_ids, chosen]  25.4 us
    all_gather x1, waiting for transfers between devices, entering_2(): pieces = jax.tree.map(lambda part: lax.all_gather(part, axis), subtotal)  24.3 us
    all_gather x1, blocking collectives, shards(): lax.all_gather(shared_hidden, 'tp', axis=1, tiled=True)  18.1 us
    reduce_scatter x1, waiting for transfers between devices, shards(): lax.psum_scatter(jnp.dot(mixed_heads, out_weight, preferred_element_type=...  12 us
  transfers between devices with their start and end apart: 6, of which 6 were waited for; matrix products, arithmetic and copies ran while one was open for 12% of the time, Pallas kernels for 0%

commit v1 on v0

--- a/solution.py
+++ b/solution.py
@@ -219,7 +219,9 @@
         * jnp.dot(expert_rows, shared_up, preferred_element_type=jnp.float32)
     ).astype(jnp.bfloat16)
     full_hidden, full_shared = (
-        lax.all_gather(hidden, "tp", axis=3, tiled=True),
+        jnp.concatenate(
+            lax.all_to_all(jnp.stack([hidden] * lax.axis_size("tp")), "tp", 0, 0), axis=3
+        ),
         lax.all_gather(shared_hidden, "tp", axis=1, tiled=True),
     )
     results = jnp.einsum(

time: 547 us -> 558 us (1.020)
  local copies, waits for them, and re-layouts: 67.4 us -> 93.4 us
  waiting for transfers between devices: 203 us -> 182 us
    all_gather x1 -> x0, waiting for transfers between devices: 43.6 us -> none  [shards(): lax.all_gather(hidden, 'tp', axis=3, tiled=True)]
    all_gather x1, waiting for transfers between devices: 5.5 us -> 40.6 us  [sent_together(): lax.all_gather(both, axis, axis=dim, tiled=True)]
    all_gather x1, waiting for transfers between devices: 24.3 us -> 0.01 us  [entering_2(): pieces = jax.tree.map(lambda part: lax.all_gather(part, axis), subtotal)]
    all_to_all x1, waiting for transfers between devices: 2.43 us -> 20.1 us  [shards(): lax.all_to_all(results, EP, split_axis=1, concat_axis=1, tiled=True)]
    all_gather x1, waiting for transfers between devices: 115 us -> 100 us  [shards(): lax.all_gather(arrived, 'tp', axis=0, tiled=True)]
    another operation x2 -> x4, local copies, waits for them, and re-layouts: 0.01 us -> 14.5 us
    reshape x0 -> x1, local copies, waits for them, and re-layouts: none -> 11.6 us  [shards(): jnp.concatenate(lax.all_to_all(jnp.stack([hidden] * lax.axis_size('tp')),...]
    all_to_all x0 -> x1, waiting for transfers between devices: none -> 8.64 us  [shards(): lax.all_to_all(jnp.stack([hidden] * lax.axis_size('tp')), 'tp', 0, 0)]
  transfers between devices with their start and end apart: 6 -> 6, of which waited for: 6 -> 5; matrix products, arithmetic and copies ran while one was open for 12% -> 17% of each run, Pallas kernels for 0% -> 0%
where the time goes in v1:
time: 558 us; the launch traced here: 551 us
  waiting for transfers between devices  182 us (33%)
  blocking collectives  170 us (30%)
  local copies, waits for them, and re-layouts  93.4 us (17%)
  matrix products  45.5 us (8%)
  other arithmetic  26.3 us (5%)
  starting transfers between devices  16.6 us (3%)
  between operations  16.4 us (3%)
    all_to_all x1, blocking collectives, shards(): lax.all_to_all(outgoing, EP, split_axis=1, concat_axis=1, tiled=True)  108 us
    all_gather x1, waiting for transfers between devices, shards(): lax.all_gather(arrived, 'tp', axis=0, tiled=True)  100 us
    all_gather x1, waiting for transfers between devices, sent_together(): lax.all_gather(both, axis, axis=dim, tiled=True)  40.6 us
    all_gather x3, blocking collectives, entering_2(): pieces = jax.tree.map(lambda part: lax.all_gather(part, axis), subtotal)  31.8 us
    scatter x1, local copies, waits for them, and re-layouts, gather_slots(): jnp.zeros((slot_count, expert_count), jnp.int32).at[slot_ids, chosen]  25.4 us
    all_to_all x1, waiting for transfers between devices, shards(): lax.all_to_all(results, EP, split_axis=1, concat_axis=1, tiled=True)  20.1 us
    all_gather x1, blocking collectives, shards(): lax.all_gather(shared_hidden, 'tp', axis=1, tiled=True)  18.6 us
    reduce_scatter x1, waiting for transfers between devices, shards(): lax.psum_scatter(jnp.dot(mixed_heads, out_weight, preferred_element_type=...  12.7 us
  transfers between devices with their start and end apart: 6, of which 5 were waited for; matrix products, arithmetic and copies ran while one was open for 17% of the time, Pallas kernels for 0%

profile of v1, /device:TPU:8, one launch (start us, length us, event | category | flops | bytes accessed | tf_op | source)
XLA Modules:
  0.0 550.5 jit_solution(14182518665546374406)
XLA Ops:
  11.3 4.8 reduce-window.6
  17.0 25.4 %scatter_fusion = s32[12,64]{1,0:T(8,128)S(1)} fusion(s32[12,64]{1,0:T(8,128)S(1)} %broadcast.459, s32[512]{0:T(512)S(1)} %bitcast.161, s32[512]{0:T(512)S(1)} %fusion.92), kind=kCustom, calls=%fused_computation.2 | custom fusion | bytes 10240 | tf_op jit(solution)/shard_map/scatter | solution.py:142
  43.6 4.3 gather_fusion
  47.8 3.7 copy.114
  51.5 108.1 %all_to_all.15 = bf16[12,64,2048]{2,0,1:T(8,128)(2,1)S(1)} all-to-all(bf16[12,64,2048]{2,0,1:T(8,128)(2,1)S(1)} %copy.114), channel_id=1, replica_groups=mesh['ep_0'=8,'ep_1'=4,'ep_2'=2,'tp'=4] {'ep_0','ep_1','ep_2'}, dimensions={1} | all-to-all | bytes 6291456 | tf_op jit(solution)/shard_map/all_to_all | solution.py:213
  170.3 9.1 %all-reduce.2 = f32[8]{0:T(128)S(1)} all-reduce(f32[8]{0:T(128)S(1)} %get-tuple-element.36), channel_id=4, replica_groups=mesh['ep_0'=8,'ep_1'=4,'ep_2'=2,'tp'=4] {'ep_1'}, use_global_device_ids=true, to_apply=%add.2 | all-reduce | flops 8 | bytes 64
  180.2 100.2 %all-gather.12.cloned.1.call-done = bf16[48,64,2048]{2,1,0:T(8,128)(2,1)} async-done(((bf16[12,64,2048]{2,1,0:T(8,128)(2,1)}), bf16[48,64,2048]{2,1,0:T(8,128)(2,1)}) %all-gather.12.cloned.1.call-update) | async-done | bytes 12582928 | tf_op jit(solution)/shard_map/all_gather | solution.py:215
  280.4 7.9 %fusion.39 = f32[48,64,256]{2,1,0:T(8,128)S(1)} fusion(bf16[48,64,2048]{2,1,0:T(8,128)(2,1)} %all-gather.12.cloned.1.call-done, bf16[1,2048,256]{2,1,0:T(8,128)(2,1)} %param.29), kind=kOutput, calls=%fused_computation.47 | convolution fusion | flops 3221225472 | bytes 16777216 | tf_op jit(solution)/shard_map/snxd,xdf->snxf/dot_general | solution.py:157
  288.9 4.1 fusion.14
  296.5 5.4 all-to-all-start.1
  301.9 16.8 %all-gather.3 = f32[8,1,2]{2,1,0:T(1,128)S(1)} all-gather(f32[1,1,2]{2,1,0:T(1,128)S(1)} %get-tuple-element.28), channel_id=1, replica_groups=mesh['ep_0'=8,'ep_1'=4,'ep_2'=2,'tp'=4] {'ep_0'}, dimensions={0}, use_global_device_ids=true | all-gather | bytes 72 | tf_op jit(solution)/shard_map/all_gather | solution.py:27
  322.5 40.6 %all-gather.8.cloned.1.call-done = bf16[512,4096]{1,0:T(8,128)(2,1)} async-done(((bf16[128,4096]{1,0:T(8,128)(2,1)}), bf16[512,4096]{1,0:T(8,128)(2,1)}) %all-gather.8.cloned.1.call-update) | async-done | bytes 4194320 | tf_op jit(solution)/shard_map/all_gather | solution.py:43
  379.4 13.0 %all_gather.44 = f32[4,2,128,128]{3,2,1,0:T(8,128)S(1)} all-gather(f32[1,2,128,128]{3,2,1,0:T(8,128)S(1)} %fusion.68), channel_id=1, replica_groups=mesh['ep_0'=8,'ep_1'=4,'ep_2'=2,'tp'=4] {'ep_1'}, dimensions={0}, use_global_device_ids=true | all-gather | bytes 655360 | tf_op jit(solution)/shard_map/all_gather | solution.py:27
  393.4 8.6 %all-to-all-done.1 = bf16[4,48,64,1,256]{4,2,1,3,0:T(8,128)(2,1)} async-done(((bf16[4,48,64,1,256]{4,2,1,3,0:T(8,128)(2,1)}), bf16[4,48,64,1,256]{4,2,1,3,0:T(8,128)(2,1)}, u32[]{:S(2)}, u32[]{:S(2)}) %all-to-all-start.1) | async-done | bytes 6291488 | tf_op jit(solution)/shard_map/all_to_all | solution.py:223
  402.0 11.6 %copy.116 = bf16[48,64,1,4,256]{4,3,1,0,2:T(4,128)(2,1)} copy(bf16[48,64,1,4,256]{4,1,0,2,3:T(8,128)(2,1)} %bitcast.44) | data formatting | bytes 12582912 | tf_op jit(solution)/shard_map/reshape | solution.py:222
  413.6 11.0 %reshape.473 = bf16[48,64,1024]{2,1,0:T(8,128)(2,1)} reshape(bf16[48,64,1,4,256]{4,3,1,0,2:T(4,128)(2,1)} %copy.116) | data formatting | bytes 12582912 | tf_op jit(solution)/shard_map/reshape.11
  424.5 6.4 %convolution_convert_fusion.1 = bf16[48,64,512]{2,1,0:T(8,128)(2,1)S(1)} fusion(bf16[48,64,1024]{2,1,0:T(8,128)(2,1)} %reshape.473, bf16[1,1024,512]{2,1,0:T(8,128)(2,1)S(1)} %copy-done), kind=kOutput, calls=%fused_computation.12 | convolution fusion | flops 3222798336 | bytes 10485760 | tf_op jit(solution)/shard_map/snxf,xfe->snxe/dot_general | solution.py:227
  434.4 10.8 %all-to-all-start.2 = ((bf16[48,64,512]{2,0,1:T(8,128)(2,1)}), bf16[48,64,512]{2,0,1:T(8,128)(2,1)}, u32[]{:S(2)}, u32[]{:S(2)}) async-start(bf16[48,64,512]{2,0,1:T(8,128)(2,1)} %copy.117), calls=%async_computation.3 | async-start | bytes 6291456 | tf_op jit(solution)/shard_map/all_to_all | solution.py:231
  465.5 18.6 %all_gather.47 = bf16[512,512]{1,0:T(8,128)(2,1)} all-gather(bf16[512,128]{1,0:T(8,128)(2,1)S(1)} %fusion.29), channel_id=1, replica_groups=mesh['ep_0'=8,'ep_1'=4,'ep_2'=2,'tp'=4] {'tp'}, dimensions={1}, use_global_device_ids=true | all-gather | bytes 655360 | tf_op jit(solution)/shard_map/all_gather | solution.py:225
  484.0 12.7 %reduce-scatter.2.cloned.1.call-done = bf16[128,2048]{1,0:T(8,128)(2,1)} async-done(((bf16[512,2048]{1,0:T(8,128)(2,1)}), bf16[128,2048]{1,0:T(8,128)(2,1)}) %reduce-scatter.2.cloned.1.call-update) | async-done | bytes 524304 | tf_op jit(solution)/shard_map/reduce_scatter | solution.py:195
  498.8 20.1 %all-to-all-done.2 = bf16[48,64,512]{2,0,1:T(8,128)(2,1)} async-done(((bf16[48,64,512]{2,0,1:T(8,128)(2,1)}), bf16[48,64,512]{2,0,1:T(8,128)(2,1)}, u32[]{:S(2)}, u32[]{:S(2)}) %all-to-all-start.2) | async-done | bytes 3145760 | tf_op jit(solution)/shard_map/all_to_all | solution.py:231
  518.9 5.3 copy.118
  524.3 9.9 %gather_fusion.1 = bf16[2048,512]{1,0:T(8,128)(2,1)S(1)} fusion(bf16[3072,512]{1,0:T(8,128)(2,1)} %bitcast.160, s32[2048]{0:T(1024)S(1)} %broadcast_clamp_fusion), kind=kCustom, calls=%fused_computation.1 | custom fusion | bytes 4202496 | tf_op jit(solution)/shard_map/gather | solution.py:233
  537.2 4.9 multiply_reduce_fusion
  (168 shorter events, 71.1 us)
Async XLA Ops:
  7.2 417.4 %copy-start = (bf16[1,1024,512]{2,1,0:T(8,128)(2,1)S(1)}, bf16[1,1024,512]{2,1,0:T(8,128)(2,1)}, u32[]{:S(2)}) copy-start(bf16[1,1024,512]{2,1,0:T(8,128)(2,1)} %param.30) | copy-start | bytes 3145732
  7.2 273.2 %all-gather.12.cloned.1.call-start = ((), (), s32[]{:S(2)}) async-start(), calls=%async_computation.7 | async-start | bytes 15728640 | tf_op jit(solution)/shard_map/all_gather | solution.py:215
  11.2 31.2 %copy-start.6 = (bf16[128,2048]{1,0:T(8,128)(2,1)S(1)}, bf16[128,2048]{1,0:T(8,128)(2,1)}, u32[]{:S(2)}) copy-start(bf16[128,2048]{1,0:T(8,128)(2,1)} %param.17) | copy-start | bytes 1572868
  11.2 31.2 %copy-start.12 = (f32[2048]{0:T(1024)S(1)}, f32[2048]{0:T(1024)}, u32[]{:S(2)}) copy-start(f32[2048]{0:T(1024)} %param.19) | copy-start | bytes 24580
  11.2 31.2 %copy-start.13 = (f32[2048]{0:T(1024)S(1)}, f32[2048]{0:T(1024)}, u32[]{:S(2)}) copy-start(f32[2048]{0:T(1024)} %param.20) | copy-start | bytes 24580
  16.0 26.4 %copy-start.7 = (bf16[128,2048]{1,0:T(8,128)(2,1)S(1)}, bf16[128,2048]{1,0:T(8,128)(2,1)}, u32[]{:S(2)}) copy-start(bf16[128,2048]{1,0:T(8,128)(2,1)} %param.18) | copy-start | bytes 1572868
  162.9 5.9 %copy-start.35 = (u32[256]{0:T(256)S(1)}, u32[256]{0:T(256)}, u32[]{:S(2)}) copy-start(u32[256]{0:T(256)} %constant.162) | copy-start | bytes 3076
  163.0 200.1 %all-gather.8.cloned.1.call-start = ((), (), s32[]{:S(2)}) async-start(), calls=%async_computation.4 | async-start | bytes 5242880 | tf_op jit(solution)/shard_map/all_gather | solution.py:43
  166.4 152.3 %copy-start.15 = (f32[2]{0:T(128)}, f32[2]{0:T(128)S(1)}, u32[]{:S(2)}) copy-start(f32[2]{0:T(128)S(1)} %get-tuple-element.39) | copy-start | bytes 28
  179.4 141.3 %copy-start.29 = (f32[8]{0:T(128)}, f32[8]{0:T(128)S(1)}, u32[]{:S(2)}) copy-start(f32[8]{0:T(128)S(1)} %iota_add_fusion.2) | copy-start | bytes 100
  180.2 108.1 %copy-start.32 = (bf16[1,2048,256]{2,1,0:T(8,128)(2,1)S(1)}, bf16[1,2048,256]{2,1,0:T(8,128)(2,1)}, u32[]{:S(2)}) copy-start(bf16[1,2048,256]{2,1,0:T(8,128)(2,1)} %param.28) | copy-start | bytes 3145732
  280.4 8.5 %copy-start.31 = (bf16[48,64,2048]{2,1,0:T(8,128)(2,1)S(1)}, bf16[48,64,2048]{2,1,0:T(8,128)(2,1)}, u32[]{:S(2)}) copy-start(bf16[48,64,2048]{2,1,0:T(8,128)(2,1)} %all-gather.12.cloned.1.call-done) | copy-start | bytes 37748740
  296.5 105.5 %all-to-all-start.1 = ((bf16[4,48,64,1,256]{4,2,1,3,0:T(8,128)(2,1)}), bf16[4,48,64,1,256]{4,2,1,3,0:T(8,128)(2,1)}, u32[]{:S(2)}, u32[]{:S(2)}) async-start(bf16[4,48,64,1,256]{4,2,1,3,0:T(8,128)(2,1)} %stack.2), calls=%async_computation.2 | async-start | bytes 12582912 | tf_op jit(solution)/shard_map/all_to_all | solution.py:223
  301.9 149.0 %all-gather.10.cloned.1.call-start = ((), (), s32[]{:S(2)}) async-start(), calls=%async_computation.5 | async-start | bytes 1179648 | tf_op jit(solution)/shard_map/all_gather | solution.py:27
  434.4 11.3 %copy-start.30 = (f32[8]{0:T(128)S(1)}, f32[8]{0:T(128)}, u32[]{:S(2)}) copy-start(f32[8]{0:T(128)} %copy-done.29) | copy-start | bytes 100
  434.4 84.5 %all-to-all-start.2 = ((bf16[48,64,512]{2,0,1:T(8,128)(2,1)}), bf16[48,64,512]{2,0,1:T(8,128)(2,1)}, u32[]{:S(2)}, u32[]{:S(2)}) async-start(bf16[48,64,512]{2,0,1:T(8,128)(2,1)} %copy.117), calls=%async_computation.3 | async-start | bytes 6291456 | tf_op jit(solution)/shard_map/all_to_all | solution.py:231
  445.3 5.6 %copy-start.19 = (f32[2]{0:T(128)S(1)}, f32[2]{0:T(128)}, u32[]{:S(2)}) copy-start(f32[2]{0:T(128)} %get-tuple-element.31) | copy-start | bytes 28
  445.3 5.6 %copy-start.20 = (f32[2]{0:T(128)S(1)}, f32[2]{0:T(128)}, u32[]{:S(2)}) copy-start(f32[2]{0:T(128)} %get-tuple-element.32) | copy-start | bytes 28
  445.3 5.6 %copy-start.21 = (f32[2]{0:T(128)S(1)}, f32[2]{0:T(128)}, u32[]{:S(2)}) copy-start(f32[2]{0:T(128)} %get-tuple-element.14) | copy-start | bytes 28
  445.4 7.3 %copy-start.16 = (f32[2]{0:T(128)S(1)}, f32[2]{0:T(128)}, u32[]{:S(2)}) copy-start(f32[2]{0:T(128)} %copy-done.15) | copy-start | bytes 28
  445.4 7.3 %copy-start.18 = (f32[8,2]{0,1:T(2,128)S(1)}, f32[8,2]{0,1:T(2,128)}, u32[]{:S(2)}) copy-start(f32[8,2]{0,1:T(2,128)} %get-tuple-element.26) | copy-start | bytes 196
  445.4 51.3 %reduce-scatter.2.cloned.1.call-start = ((), (), s32[]{:S(2)}) async-start(), calls=%async_computation.6 | async-start | bytes 2621440 | tf_op jit(solution)/shard_map/reduce_scatter | solution.py:195
  448.6 5.8 %copy-start.1 = (f32[512,2,64]{2,0,1:T(8,128)S(1)}, f32[512,2,64]{2,0,1:T(8,128)}, u32[]{:S(2)}) copy-start(f32[512,2,64]{2,0,1:T(8,128)} %get-tuple-element.4) | copy-start | bytes 786436
  448.6 5.8 %copy-start.17 = (f32[64,2]{0,1:T(2,128)S(1)}, f32[64,2]{0,1:T(2,128)}, u32[]{:S(2)}) copy-start(f32[64,2]{0,1:T(2,128)} %get-tuple-element.24) | copy-start | bytes 1540
  (19 other events, 70.2 us)
Sparse Core Ops, SparseCore 0:
  163.1 117.2 all-gather.11
  282.8 80.2 all-gather.7
  393.3 39.3 all-gather.9
  460.5 36.1 reduce-scatter.1
